TPU v7x, 32 devices: a whole 2x2x4 slice. The times are simulated.
32 devices in a mesh: kv: 8 (over z, y), tp: 4 (over x, core).
Axes of the slice: x: 2, y: 2, z: 4, core: 2. Of those that a mesh axis runs over, the one named last changes fastest.
Arguments:
- query_rows: bfloat16 [16384, 1536], P('kv', 'tp'), may hold values from -6 to 6
- key_rows: bfloat16 [16384, 1536], P('kv', 'tp'), may hold values from -6 to 6
- value_rows: bfloat16 [16384, 1536], P('kv', 'tp'), may hold values from -6 to 6
- log_sums: float32 [12, 16384], P('tp', 'kv'), may hold values from 5.5 to 7.5
- cotangent: bfloat16 [16384, 1536], P('kv', 'tp'), may hold values from -24 to 24
- layer_input: bfloat16 [16384, 4096], P('kv', 'tp'), may hold values from -0.29882812 to 0.29882812
- chosen: int32 [12, 512, 12], P('tp'), may hold values from -1 to 447, as said below
Outputs:
- grad_queries: bfloat16 [16384, 1536], P('kv', 'tp')
- grad_keys: float32 [16384, 1536], P('kv', 'tp')
- grad_values: float32 [16384, 1536], P('kv', 'tp')
- grad_weight: float32 [4096, 1536], P(('tp', 'kv'))
Inputs may be any that keep to these rules, and one draw needn't show every extreme that they name: `chosen`: for query block i, write j = i // 64. Every entry other than -1 names a block below j * 64; the entries of a row are distinct, the -1 entries stand last, and a row has exactly min(12, 2 * min(j, 7)) entries other than -1. For one head, the rows with the same j name at most 2 distinct blocks of any one span; for j >= 1 the span j - 1 gives exactly 2 blocks, named by every such row.
All inputs are finite; a program needn't handle non-finite values.
Results may differ from a plain program's by a relative error of at most 0.007.
Values may be sent and summed in bfloat16 or wider, within the bound.
A program may use at most 192 MiB of HBM per device.

v0:
```python
import functools

import jax
import jax.numpy as jnp
from jax import lax
from jax.experimental import pallas as pl
from jax.experimental.pallas import tpu as pltpu
from jax.sharding import PartitionSpec as P

HEAD_DIM = 128
KEY_BLOCK = 32
CAP = 2
SUB = 128
NEVER = -1e30
LOG2E = 1.4426950408889634

MESH = pl.DeviceIdType.MESH
NT = (((1,), (1,)), ((), ()))
NN = (((1,), (0,)), ((), ()))
TN = (((0,), (0,)), ((), ()))


def dot(a, b, dims):
    return lax.dot_general(a, b, dims, preferred_element_type=jnp.float32)


def flip(place, bit):
    return place + bit - 2 * bit * lax.rem(lax.div(place, bit), 2)


def chunk_plan(heads):
    chunks = []
    for head in range(heads):
        chunks.append((("own", head), ("came", head)))
    return chunks


def step_plan(heads):
    last = heads - 1
    plan = []
    for head in range(heads):
        plan.append(("attend", head))
        if head:
            plan.append(("product", head - 1))
    plan.append(("relay", 0))
    plan.append(("product", last))
    for head in range(1, heads):
        plan.append(("relay", head))
    return plan


class Kernel:
    def __init__(self, spans, tp_count, heads, rows, features):
        self.spans, self.tp_count, self.heads = spans, tp_count, heads
        self.rows, self.features = rows, features
        self.far_rows = (spans - 1) * CAP * KEY_BLOCK
        self.tile = 256 if self.far_rows <= 512 else SUB
        self.tiles = rows // self.tile
        self.slice = features // spans
        self.pieces = spans // 2
        self.chunks = chunk_plan(heads)
        self.plan = step_plan(heads)
        self.stages = spans.bit_length() - 1

    def scratch(self):
        spans, heads, rows = self.spans, self.heads, self.rows
        span_rows = CAP * KEY_BLOCK
        wide = heads * HEAD_DIM
        bf, f32 = jnp.bfloat16, jnp.float32
        dma = pltpu.SemaphoreType.DMA
        out = dict(
            query=pltpu.VMEM((rows, wide), bf),
            key=pltpu.VMEM((rows, wide), bf),
            value=pltpu.VMEM((rows, wide), bf),
            cot=pltpu.VMEM((rows, wide), bf),
            layer=pltpu.VMEM((rows, self.features), bf),
            turned=pltpu.VMEM((spans, 2, self.slice, rows), bf),
            far=pltpu.VMEM((heads, spans, 2, span_rows, HEAD_DIM), bf),
            back=pltpu.VMEM((heads, spans, 2, span_rows, HEAD_DIM), bf),
            acc=pltpu.VMEM((2, self.far_rows, HEAD_DIM), f32),
            dq=pltpu.VMEM((heads, rows, HEAD_DIM), bf),
            came=pltpu.VMEM((heads, rows, HEAD_DIM), bf),
            dkv=pltpu.VMEM((heads, 2, rows, HEAD_DIM), f32),
            load_sem=dma((6,)),
            store_sem=dma((heads, 3)),
            far_send=dma((heads, spans)),
            far_recv=dma((heads, spans)),
            back_send=dma((heads, spans)),
            back_recv=dma((heads, spans)),
            turn_send=dma((spans,)),
            turn_recv=dma((spans,)),
            dq_send=dma((heads, self.tiles)),
            dq_recv=dma((heads, self.tiles)),
        )
        count = len(self.chunks)
        for c, chunk in enumerate(self.chunks):
            width = HEAD_DIM * len(chunk)
            out[f"part{c}"] = pltpu.VMEM((self.pieces, 2, 2 * self.slice, width), f32)
            left = self.pieces
            for stage in range(self.stages):
                give = left if stage == 0 else left // 2
                shape = (give, 2 * self.slice, width)
                out[f"give{c}_{stage}"] = pltpu.VMEM(shape, bf)
                out[f"got{c}_{stage}"] = pltpu.VMEM(shape, bf)
                out[f"give_sem{c}_{stage}"] = dma((give,))
                out[f"got_sem{c}_{stage}"] = dma((give,))
                left = give if stage == 0 else left - give
            out[f"sum{c}"] = pltpu.VMEM((2, self.slice, width), f32)
            out[f"other{c}"] = pltpu.VMEM((self.slice, width), f32)
        out["sum_send"] = dma((count,))
        out["sum_recv"] = dma((count,))
        return out

    def body(self, names, *refs):
        fixed = (
            "bias", "picked", "query_in", "key_in", "value_in", "cot_in", "layer_in", "dq_out", "dk_out", "dv_out", "home", "weight",
        )
        for name, ref in zip(fixed + names, refs, strict=True):
            setattr(self, name, ref)
        self.me = lax.axis_index("kv")
        self.tp = lax.axis_index("tp")
        self.side = self.tp_count // 2
        self.start()
        for head in range(self.heads):
            self.send_far(head)
        self.turn()
        for kind, index in self.plan:
            getattr(self, kind)(index)
        self.finish()


    def load(self, which):
        pairs = (
            (self.key_in, self.key),
            (self.value_in, self.value),
            (self.query_in, self.query),
            (self.cot_in, self.cot),
            (self.layer_in, self.layer),
        )
        src, dst = pairs[which]
        return pltpu.make_async_copy(src, dst, self.load_sem.at[which])

    def remote(self, src, dst, send, recv, **to):
        return pltpu.make_async_remote_copy(
            src_ref=src, dst_ref=dst, send_sem=send, recv_sem=recv,
            device_id=to, device_id_type=MESH,
        )

    def far_copy(self, head, to, sender):
        return self.remote(
            self.picked.at[to, head], self.far.at[head, sender],
            self.far_send.at[head, to], self.far_recv.at[head, sender], kv=to,
        )

    def back_copy(self, head, to, sender):
        return self.remote(
            self.back.at[head, to], self.home.at[sender, head],
            self.back_send.at[head, to], self.back_recv.at[head, sender], kv=to,
        )

    def turn_copy(self, place):
        return self.remote(
            self.turned.at[place, 0], self.turned.at[place, 1],
            self.turn_send.at[place], self.turn_recv.at[place], tp=flip(self.tp, 1),
        )

    def dq_copy(self, head, tile):
        rows = pl.ds(pl.multiple_of(tile * self.tile, self.tile), self.tile)
        return self.remote(
            self.dq.at[head, rows], self.came.at[head, rows],
            self.dq_send.at[head, tile], self.dq_recv.at[head, tile],
            tp=flip(self.tp, self.side),
        )

    def give_copy(self, c, stage, slot):
        return self.remote(
            getattr(self, f"give{c}_{stage}").at[slot],
            getattr(self, f"got{c}_{stage}").at[slot],
            getattr(self, f"give_sem{c}_{stage}").at[slot],
            getattr(self, f"got_sem{c}_{stage}").at[slot],
            kv=flip(self.me, 2**stage),
        )

    def sum_copy(self, c):
        return self.remote(
            getattr(self, f"sum{c}").at[1], getattr(self, f"other{c}"),
            self.sum_send.at[c], self.sum_recv.at[c], tp=flip(self.tp, 1),
        )

    def result_copies(self, head):
        columns = pl.ds(head * HEAD_DIM, HEAD_DIM)
        pairs = (
            (self.dq.at[head], self.dq_out),
            (self.dkv.at[head, 0], self.dk_out),
            (self.dkv.at[head, 1], self.dv_out),
        )
        return [
            pltpu.make_async_copy(src, dst.at[:, columns], self.store_sem.at[head, i])
            for i, (src, dst) in enumerate(pairs)
        ]


    def start(self):
        for which in range(5):
            self.load(which).start()
        barrier = pltpu.get_barrier_semaphore()

        def greet(step, carry):
            to = lax.rem(self.me + step, self.spans)
            pl.semaphore_signal(barrier, inc=1, device_id={"kv": to}, device_id_type=MESH)
            return carry

        lax.fori_loop(1, self.spans, greet, 0)
        for bit in (1, self.side):
            pl.semaphore_signal(
                barrier, inc=1, device_id={"tp": flip(self.tp, bit)}, device_id_type=MESH
            )

        def blank(span, carry):
            for head in range(self.heads):
                self.far[head, span] = jnp.zeros(self.far.shape[2:], jnp.bfloat16)
            return carry

        lax.fori_loop(self.me, self.spans, blank, 0)
        pl.semaphore_wait(barrier, self.spans + 1)

    def send_far(self, head):
        def send(to, carry):
            self.far_copy(head, to, self.me).start()
            return carry

        lax.fori_loop(self.me + 1, self.spans, send, 0)

    def turn(self):
        self.load(4).wait()
        group = HEAD_DIM // self.slice
        step_rows = 512

        def one(g, carry):
            columns = pl.ds(pl.multiple_of(g * HEAD_DIM, HEAD_DIM), HEAD_DIM)
            for at in range(0, self.rows, step_rows):
                block = self.layer[at : at + step_rows, columns].T
                for j in range(group):
                    self.turned[g * group + j, 0, :, at : at + step_rows] = block[
                        j * self.slice : (j + 1) * self.slice
                    ]

            @pl.when(g > 0)
            def _():
                for j in range(group):
                    self.turn_copy((g - 1) * group + j).start()

            return carry

        last = self.features // HEAD_DIM
        lax.fori_loop(0, last, one, 0)
        for which in range(4):
            self.load(which).wait()
        for j in range(group):
            self.turn_copy((last - 1) * group + j).start()

    def attend(self, head):
        def arrived(span, carry):
            self.far_copy(head, self.me, span).wait_recv()
            return carry

        lax.fori_loop(0, self.me, arrived, 0)
        lax.fori_loop(0, self.tiles, functools.partial(self.attend_tile, head), 0)
        self.dq_copy(head, self.tiles - 1).start()
        for copy in self.result_copies(head):
            copy.start()
        scale = HEAD_DIM ** (-0.5)
        spans = self.spans
        shape = (spans - 1, CAP * KEY_BLOCK, HEAD_DIM)
        self.back[head, : spans - 1, 0] = (scale * self.acc[0]).astype(jnp.bfloat16).reshape(shape)
        self.back[head, : spans - 1, 1] = self.acc[1].astype(jnp.bfloat16).reshape(shape)

        def send(to, carry):
            self.back_copy(head, to, self.me).start()
            return carry

        lax.fori_loop(0, self.me, send, 0)

    def attend_tile(self, head, step, carry):
        tile, spans, far_rows = self.tile, self.spans, self.far_rows
        scale = HEAD_DIM ** (-0.5)
        columns = slice(head * HEAD_DIM, (head + 1) * HEAD_DIM)
        rows = pl.ds(pl.multiple_of(step * tile, tile), tile)
        query = self.query[rows, columns]
        key = self.key[rows, columns]
        value = self.value[rows, columns]
        cot = self.cot[rows, columns]
        far_k = self.far[head, : spans - 1, 0].reshape(far_rows, HEAD_DIM)
        far_v = self.far[head, : spans - 1, 1].reshape(far_rows, HEAD_DIM)
        far_bias = self.bias[head, : (spans - 1) * CAP, rows]
        sums = self.bias[head, spans * CAP :, rows]
        far_bias = jnp.broadcast_to(
            far_bias[:, None, :], ((spans - 1) * CAP, KEY_BLOCK, tile)
        ).reshape(far_rows, tile)
        j = lax.broadcasted_iota(jnp.int32, (SUB, tile), 0)
        t = lax.broadcasted_iota(jnp.int32, (SUB, tile), 1) % SUB
        own_ok = (j // KEY_BLOCK == t // KEY_BLOCK) & (j <= t)
        own_bias = jnp.where(own_ok, 0.0, NEVER) + sums[0:1]

        parts = [slice(at, at + SUB) for at in range(0, tile, SUB)]
        own_s = jnp.concatenate([dot(key[r, :], query[r, :], NT) for r in parts], axis=1)
        own_g = jnp.concatenate([dot(value[r, :], cot[r, :], NT) for r in parts], axis=1)
        far_s = dot(far_k, query, NT)
        far_g = dot(far_v, cot, NT)
        far_p = jnp.exp2(far_s * (scale * LOG2E) + far_bias)
        own_p = jnp.exp2(own_s * (scale * LOG2E) + own_bias)
        row_dots = jnp.sum(far_p * far_g, axis=0, keepdims=True) + jnp.sum(
            own_p * own_g, axis=0, keepdims=True
        )
        far_d = (far_p * (far_g - row_dots)).astype(jnp.bfloat16)
        own_d = (own_p * (own_g - row_dots)).astype(jnp.bfloat16)
        far_low = far_p.astype(jnp.bfloat16)
        own_low = own_p.astype(jnp.bfloat16)

        far_q = dot(far_d, far_k, TN)
        for r in parts:
            dq = far_q[r, :] + dot(own_d[:, r], key[r, :], TN)
            here = pl.ds(pl.multiple_of(step * tile + r.start, SUB), SUB)
            self.dq[head, here, :] = (scale * dq).astype(jnp.bfloat16)
            self.dkv[head, 0, here, :] = scale * dot(own_d[:, r], query[r, :], NN)
            self.dkv[head, 1, here, :] = dot(own_low[:, r], cot[r, :], NN)
        step_k = dot(far_d, query, NN)
        step_v = dot(far_low, cot, NN)

        @pl.when(step == 0)
        def _():
            self.acc[0] = step_k
            self.acc[1] = step_v

        @pl.when(step > 0)
        def _():
            self.acc[0] += step_k
            self.acc[1] += step_v
            self.dq_copy(head, step - 1).start()

        return carry

    def source(self, kind, head):
        return (self.dq if kind == "own" else self.came)[head]

    def place_of(self, slot):
        left = self.pieces - 1 - slot
        place = self.me
        for bit in range(1, self.stages):
            on = lax.rem(lax.div(left, 2 ** (self.stages - 1 - bit)), 2)
            place = place + on * (flip(self.me, 2**bit) - self.me)
        return place

    def product(self, c):
        chunk = self.chunks[c]
        part = getattr(self, f"part{c}")
        give = getattr(self, f"give{c}_0")
        for kind, head in chunk:
            if kind == "came":

                def arrived(tile, carry, head=head):
                    self.dq_copy(head, tile).wait_recv()
                    return carry

                lax.fori_loop(0, self.tiles, arrived, 0)
        if c == 0:

            def turned(place, carry):
                self.turn_copy(place).wait_recv()
                return carry

            lax.fori_loop(0, self.spans, turned, 0)
        bit = lax.rem(self.me, 2)

        def one(slot, carry):
            pair = lax.div(self.place_of(slot), 2) * 2
            left = self.turned[pl.ds(pair, 2)].reshape(4 * self.slice, self.rows)
            right = jnp.concatenate([self.source(*s) for s in chunk], axis=1)
            part[slot] = dot(left, right, NN).reshape(part.shape[1:])
            give[slot] = part[slot, 1 - bit].astype(jnp.bfloat16)
            self.give_copy(c, 0, slot).start()
            return carry

        lax.fori_loop(0, self.pieces, one, 0)

    def relay(self, c):
        part = getattr(self, f"part{c}")
        bit = lax.rem(self.me, 2)
        low, ranges = 0, []
        for stage in range(1, self.stages):
            half = (self.pieces - low) // 2
            ranges.append((stage, low, half))
            low += half

        def total(slot):
            self.give_copy(c, 0, slot).wait_recv()
            value = part[slot, bit] + getattr(self, f"got{c}_0")[slot].astype(jnp.float32)
            for stage, first, half in ranges:
                if slot >= first + half:
                    at = slot - half - first
                    self.give_copy(c, stage, at).wait_recv()
                    got = getattr(self, f"got{c}_{stage}")
                    value = value + got[at].astype(jnp.float32)
                else:
                    break
            return value

        for stage, first, half in ranges:
            for slot in range(first, first + half):
                getattr(self, f"give{c}_{stage}")[slot - first] = total(slot).astype(jnp.bfloat16)
                self.give_copy(c, stage, slot - first).start()
        final = getattr(self, f"sum{c}")
        final[...] = total(self.pieces - 1).reshape(final.shape)
        self.sum_copy(c).start()
        for at, (kind, head) in enumerate(self.chunks[c]):
            self.put(self.tp, kind, head, final[0, :, at * HEAD_DIM : (at + 1) * HEAD_DIM])

    def put(self, tp, kind, head, block):
        if kind == "came":
            tp = flip(tp, self.side)
        column = pl.multiple_of((tp * self.heads + head) * HEAD_DIM, HEAD_DIM)
        self.weight[:, pl.ds(column, HEAD_DIM)] = block

    def finish(self):
        for c, chunk in enumerate(self.chunks):
            self.sum_copy(c).wait_recv()
            other = getattr(self, f"other{c}")
            for at, (kind, head) in enumerate(chunk):
                self.put(
                    flip(self.tp, 1), kind, head, other[:, at * HEAD_DIM : (at + 1) * HEAD_DIM]
                )
            self.sum_copy(c).wait_send()
            for stage in range(self.stages):
                for slot in range(getattr(self, f"give{c}_{stage}").shape[0]):
                    self.give_copy(c, stage, slot).wait_send()

        def turned(place, carry):
            self.turn_copy(place).wait_send()
            return carry

        lax.fori_loop(0, self.spans, turned, 0)
        for head in range(self.heads):

            def later(span, carry, head=head):
                self.far_copy(head, span, self.me).wait_send()
                self.back_copy(head, self.me, span).wait_recv()
                return carry

            lax.fori_loop(self.me + 1, self.spans, later, 0)

            def earlier(span, carry, head=head):
                self.back_copy(head, span, self.me).wait_send()
                return carry

            lax.fori_loop(0, self.me, earlier, 0)

            def sent(tile, carry, head=head):
                self.dq_copy(head, tile).wait_send()
                return carry

            lax.fori_loop(0, self.tiles, sent, 0)
            for copy in self.result_copies(head):
                copy.wait()


def whole_step(bias, picked, query, key, value, cot, layer, tp_count):
    spans, heads = picked.shape[:2]
    rows = query.shape[0]
    plan = Kernel(spans, tp_count, heads, rows, layer.shape[1])
    scratch = plan.scratch()
    names = tuple(scratch)
    vmem = pl.BlockSpec(memory_space=pltpu.VMEM)
    hbm = pl.BlockSpec(memory_space=pl.ANY)
    wide = heads * HEAD_DIM
    return pl.pallas_call(
        functools.partial(plan.body, names),
        out_shape=(
            jax.ShapeDtypeStruct((rows, wide), jnp.bfloat16),
            jax.ShapeDtypeStruct((rows, wide), jnp.float32),
            jax.ShapeDtypeStruct((rows, wide), jnp.float32),
            jax.ShapeDtypeStruct((spans, heads, 2, CAP * KEY_BLOCK, HEAD_DIM), jnp.bfloat16),
            jax.ShapeDtypeStruct((plan.slice, tp_count * wide), jnp.float32),
        ),
        in_specs=[vmem] + [hbm] * 6,
        out_specs=(hbm, hbm, hbm, hbm, vmem),
        scratch_shapes=list(scratch.values()),
        compiler_params=pltpu.CompilerParams(
            collective_id=0, has_side_effects=True, vmem_limit_bytes=67043328
        ),
        name="whole_step",
    )(bias, picked, query, key, value, cot, layer)


def prepare_body(chosen, sums, key_in, value_in, ids, picked, bias, key, value, found, marks, sem, mark_sem):
    loads = [
        pltpu.make_async_copy(src, dst, sem.at[i])
        for i, (src, dst) in enumerate(((key_in, key), (value_in, value)))
    ]
    for load in loads:
        load.start()
    spans, heads = picked.shape[:2]
    rows = sums.shape[1]
    blocks = rows // KEY_BLOCK
    entries = chosen.shape[2]
    first = lax.axis_index("kv") * blocks
    for head in range(heads):
        lists = chosen[head] - first
        mine = (lists >= 0) & (lists < blocks)
        low = jnp.where(mine, lists, blocks).reshape(spans, blocks, entries)
        high = jnp.where(mine, lists, 0).reshape(spans, blocks, entries)
        low = jnp.min(jnp.min(low, axis=1), axis=1, keepdims=True)
        high = jnp.max(jnp.max(high, axis=1), axis=1, keepdims=True)
        low = jnp.where(low == blocks, 0, low)
        lane = lax.broadcasted_iota(jnp.int32, (spans, 128), 1)
        found[head] = jnp.where(lane == 0, low, high)
    copy = pltpu.make_async_copy(found, marks, mark_sem)
    copy.start()

    none = spans * blocks
    row = lax.broadcasted_iota(jnp.int32, (blocks, rows), 0)
    spread = jnp.where(
        lax.broadcasted_iota(jnp.int32, (blocks, rows), 1) // KEY_BLOCK == row, 1.0, 0.0
    ).astype(jnp.bfloat16)
    for head in range(heads):
        own = chosen[head, pl.ds(pl.multiple_of(first, blocks), blocks), :]
        lane = lax.broadcasted_iota(jnp.int32, (1, spans * CAP), 1)
        wanted = jnp.full((1, spans * CAP), -2, jnp.int32)
        for span in range(spans):
            inside = (own >= span * blocks) & (own < (span + 1) * blocks)
            low = jnp.min(jnp.where(inside, own, none), axis=0, keepdims=True)
            low = jnp.min(low, axis=1, keepdims=True)
            high = jnp.max(jnp.where(inside, own, -2), axis=0, keepdims=True)
            high = jnp.max(high, axis=1, keepdims=True)
            high = jnp.where(high == low, -2, high)
            wanted = jnp.where(lane == span * CAP, low, wanted)
            wanted = jnp.where(lane == span * CAP + 1, high, wanted)
        hit = own[:, 0:1] == wanted
        for entry in range(1, entries):
            hit = hit | (own[:, entry : entry + 1] == wanted)
        hit = jnp.where(hit, 1.0, 0.0).astype(jnp.bfloat16)
        used = dot(hit, spread, TN)
        minus = sums[head : head + 1, :] * -LOG2E
        bias[head, : spans * CAP, :] = jnp.where(used > 0.5, minus, NEVER)
        bias[head, spans * CAP :, :] = jnp.broadcast_to(minus, (8, rows))

    copy.wait()
    for load in loads:
        load.wait()

    def one(span, carry):
        for head in range(heads):
            columns = slice(head * HEAD_DIM, (head + 1) * HEAD_DIM)
            for slot in range(CAP):
                block = marks[head, span, slot]
                ids[slot, head * spans + span] = block
                at = pl.ds(pl.multiple_of(block * KEY_BLOCK, KEY_BLOCK), KEY_BLOCK)
                to = slice(slot * KEY_BLOCK, (slot + 1) * KEY_BLOCK)
                picked[span, head, 0, to, :] = key[at, columns]
                picked[span, head, 1, to, :] = value[at, columns]
        return carry

    lax.fori_loop(0, spans, one, 0)


def prepare(chosen, sums, key, value, spans):
    heads, rows = sums.shape
    vmem = pl.BlockSpec(memory_space=pltpu.VMEM)
    smem = pl.BlockSpec(memory_space=pltpu.SMEM)
    hbm = pl.BlockSpec(memory_space=pl.ANY)
    return pl.pallas_call(
        prepare_body,
        out_shape=(
            jax.ShapeDtypeStruct((CAP, heads * spans), jnp.int32),
            jax.ShapeDtypeStruct((spans, heads, 2, CAP * KEY_BLOCK, HEAD_DIM), jnp.bfloat16),
            jax.ShapeDtypeStruct((heads, spans * CAP + 8, rows), jnp.float32),
        ),
        in_specs=[vmem, vmem, hbm, hbm],
        out_specs=(smem, vmem, vmem),
        scratch_shapes=[
            pltpu.VMEM(key.shape, key.dtype),
            pltpu.VMEM(value.shape, value.dtype),
            pltpu.VMEM((heads, spans, 128), jnp.int32),
            pltpu.SMEM((heads, spans, 128), jnp.int32),
            pltpu.SemaphoreType.DMA((2,)),
            pltpu.SemaphoreType.DMA,
        ],
        name="prepare_blocks",
    )(chosen, sums, key, value)


def land_body(ids_ref, own_k, own_v, home, out_k, out_v):
    spans = home.shape[0]
    head = pl.program_id(0)
    out_k[...] = own_k[...]
    out_v[...] = own_v[...]

    def one(span, carry):
        for slot in range(CAP):
            start = pl.multiple_of(ids_ref[slot, head * spans + span] * KEY_BLOCK, KEY_BLOCK)
            rows = pl.ds(start, KEY_BLOCK)
            at = slice(slot * KEY_BLOCK, (slot + 1) * KEY_BLOCK)
            out_k[rows, :] += home[span, 0, 0, at, :].astype(jnp.float32)
            out_v[rows, :] += home[span, 0, 1, at, :].astype(jnp.float32)
        return carry

    lax.fori_loop(lax.axis_index("kv") + 1, spans, one, 0)


def land(ids, own_k, own_v, home):
    spans, heads = home.shape[:2]
    rows = own_k.shape[0]
    whole = jax.ShapeDtypeStruct((rows, heads * HEAD_DIM), jnp.float32)
    column = pl.BlockSpec((rows, HEAD_DIM), lambda h: (0, h))
    return pl.pallas_call(
        land_body,
        grid=(heads,),
        out_shape=(whole, whole),
        in_specs=[
            pl.BlockSpec(memory_space=pltpu.SMEM),
            column,
            column,
            pl.BlockSpec((spans, 1) + home.shape[2:], lambda h: (0, h, 0, 0, 0)),
        ],
        out_specs=(column, column),
        name="land_blocks",
    )(ids, own_k, own_v, home)


def local(query_rows, key_rows, value_rows, log_sums, cotangent, layer_input, chosen):
    kv_count = lax.axis_size("kv")
    tp_count = lax.axis_size("tp")
    ids, picked, bias = prepare(chosen, log_sums, key_rows, value_rows, kv_count)
    dq, own_k, own_v, home, weight = whole_step(
        bias, picked, query_rows, key_rows, value_rows, cotangent, layer_input, tp_count
    )
    grad_keys, grad_values = land(ids, own_k, own_v, home)
    return dq, grad_keys, grad_values, weight


def solution(mesh):
    placed = (
        P("kv", "tp"),
        P("kv", "tp"),
        P("kv", "tp"),
        P("tp", "kv"),
        P("kv", "tp"),
        P("kv", "tp"),
        P("tp", None, None),
    )
    return jax.shard_map(
        local,
        mesh=mesh,
        in_specs=placed,
        out_specs=(P("kv", "tp"), P("kv", "tp"), P("kv", "tp"), P(("tp", "kv"), None)),
        check_vma=False,
    )
```

profile of v0, /device:TPU:0, one launch (start us, length us, event | category | flops | bytes accessed | tf_op | source)
XLA Modules:
  0.0 102.4 jit_solution(3873618999751179391)
XLA Ops:
  0.6 2.1 %copy.11.chosen = s32[3,512,12]{2,1,0:T(8,128)} copy(s32[3,512,12]{1,2,0:T(8,128)} %param.13) | data formatting | bytes 147456 | tf_op args[6]
  2.7 4.5 %prepare_blocks.1 = (s32[2,24]{1,0:T(2,128)}, bf16[8,3,2,64,128]{4,3,2,1,0:T(8,128)(2,1)}, f32[3,24,2048]{2,1,0:T(8,128)}) custom-call(s32[3,512,12]{2,1,0:T(8,128)} %copy.11.chosen, f32[3,2048]{1,0:T(4,128)} %sums.1, bf16[2048,384]{1,0:T(8,128)(2,1)} %refs_3_.1, bf16[2048,384]{1,0:T(8,128)(2,1)} %refs_4_.1), custom_call_target="tpu_custom_call" | custom-call | tf_op jit(solution)/shard_map/prepare_blocks/pallas_call | solution.py:570
  7.2 85.8 %whole_step.1 = (bf16[2048,384]{1,0:T(8,128)(2,1)}, f32[2048,384]{1,0:T(8,128)}, f32[2048,384]{1,0:T(8,128)}, bf16[8,3,2,64,128]{4,3,2,1,0:T(8,128)(2,1)}, f32[128,1536]{1,0:T(8,128)}) custom-call(f32[3,24,2048]{2,1,0:T(8,128)} %get-tuple-element.14.refs_0_, bf16[8,3,2,64,128]{4,3,2,1,0:T(8,128)(2,1)} %get-tuple-element.15.refs_1_, ...), custom_call_target="tpu_custom_call" | custom-call | tf_op jit(solution)/shard_map/whole_step/pallas_call | solution.py:475
  93.0 0.0 copy-start
  93.0 6.8 %land_blocks.1 = (f32[2048,384]{1,0:T(8,128)}, f32[2048,384]{1,0:T(8,128)}) custom-call(s32[2,24]{1,0:T(2,128)} %get-tuple-element.17.ids_ref, f32[2048,384]{1,0:T(8,128)} %get-tuple-element.18.own_k, f32[2048,384]{1,0:T(8,128)} %get-tuple-element.19.own_v, bf16[8,3,2,64,128]{4,3,2,1,0:T(8,128)(2,1)} %get-tuple-element.20.home), custom_call_target="tpu_custom_call" | custom-call | tf_op jit(solution)/shard_map/land_blocks/pallas_call | solution.py:614
  99.8 0.0 copy-done
  99.8 0.0 copy-start.1
  99.8 1.1 %copy.14 = bf16[2048,384]{1,0:T(8,128)(2,1)} copy(bf16[2048,384]{1,0:T(8,128)(2,1)S(1)} %copy-done) | data formatting | bytes 3145728
  101.0 0.5 copy-done.1
  101.5 0.9 copy.15
Async XLA Ops:
  93.0 6.8 %copy-start = (bf16[2048,384]{1,0:T(8,128)(2,1)S(1)}, bf16[2048,384]{1,0:T(8,128)(2,1)}, u32[]{:S(2)}) copy-start(bf16[2048,384]{1,0:T(8,128)(2,1)} %get-tuple-element.28) | copy-start | bytes 4718596
  99.8 1.7 %copy-start.1 = (f32[128,1536]{1,0:T(8,128)S(1)}, f32[128,1536]{1,0:T(8,128)}, u32[]{:S(2)}) copy-start(f32[128,1536]{1,0:T(8,128)} %get-tuple-element.31) | copy-start | bytes 2359300
where the time goes:
time: 103 us; the launch traced here: 102 us
  Pallas kernels  97.1 us (94%)
  local copies, waits for them, and re-layouts  4.6 us (4%)
    pallas_call x1, Pallas kernels, whole_step(): pl.pallas_call(functools.partial(plan.body, names), out_shape=(jax.ShapeD...  85.8 us
    pallas_call x1, Pallas kernels, land(): pl.pallas_call(land_body, grid=(heads,), out_shape=(whole, whole), in_spe...  6.8 us
    unnamed x7, local copies, waits for them, and re-layouts  4.6 us
    pallas_call x1, Pallas kernels, prepare(): pl.pallas_call(prepare_body, out_shape=(jax.ShapeDtypeStruct((CAP, heads...  4.47 us

commit v1 on v0

--- a/solution.py
+++ b/solution.py
@@ -29,24 +29,28 @@
 
 
 def chunk_plan(heads):
-    chunks = []
-    for head in range(heads):
-        chunks.append((("own", head), ("came", head)))
-    return chunks
+    own = [("own", head) for head in range(heads)]
+    came = [("came", head) for head in range(heads)]
+    return [[one] for one in own[:-1]] + [[own[-1], came[0]]] + [[one] for one in came[1:]]
 
 
 def step_plan(heads):
-    last = heads - 1
     plan = []
     for head in range(heads):
-        plan.append(("attend", head))
+        plan += [("attend", head), ("product", head), ("send_home", head)]
         if head:
-            plan.append(("product", head - 1))
-    plan.append(("relay", 0))
-    plan.append(("product", last))
-    for head in range(1, heads):
-        plan.append(("relay", head))
-    return plan
+            plan.append(("first", head - 1))
+    plan += [("rest", chunk) for chunk in range(heads - 2)]
+    last = 2 * heads - 2
+    for chunk in range(heads, last + 1):
+        plan += [("product", chunk), ("first", chunk - 1)]
+        if chunk == heads:
+            plan.append(("rest", heads - 2))
+            plan += [("settle", early) for early in range(heads - 1)]
+        else:
+            plan.append(("settle", chunk - 2))
+        plan.append(("rest", chunk - 1))
+    return plan + [("first", last), ("settle", last - 1), ("rest", last), ("settle", last)]
 
 
 class Kernel:
@@ -54,7 +58,7 @@
         self.spans, self.tp_count, self.heads = spans, tp_count, heads
         self.rows, self.features = rows, features
         self.far_rows = (spans - 1) * CAP * KEY_BLOCK
-        self.tile = 256 if self.far_rows <= 512 else SUB
+        self.tile = 1024 if self.far_rows <= 512 else 256
         self.tiles = rows // self.tile
         self.slice = features // spans
         self.pieces = spans // 2
@@ -78,11 +82,13 @@
             far=pltpu.VMEM((heads, spans, 2, span_rows, HEAD_DIM), bf),
             back=pltpu.VMEM((heads, spans, 2, span_rows, HEAD_DIM), bf),
             acc=pltpu.VMEM((2, self.far_rows, HEAD_DIM), f32),
+            key_turned=pltpu.VMEM((HEAD_DIM, self.far_rows), bf),
+            bias=pltpu.VMEM((heads, spans * CAP + 8, rows), f32),
             dq=pltpu.VMEM((heads, rows, HEAD_DIM), bf),
             came=pltpu.VMEM((heads, rows, HEAD_DIM), bf),
             dkv=pltpu.VMEM((heads, 2, rows, HEAD_DIM), f32),
             load_sem=dma((6,)),
-            store_sem=dma((heads, 3)),
+            store_sem=dma((heads, 2)),
             far_send=dma((heads, spans)),
             far_recv=dma((heads, spans)),
             back_send=dma((heads, spans)),
@@ -113,7 +119,7 @@
 
     def body(self, names, *refs):
         fixed = (
-            "bias", "picked", "query_in", "key_in", "value_in", "cot_in", "layer_in", "dq_out", "dk_out", "dv_out", "home", "weight",
+            "chosen", "sums", "picked", "query_in", "key_in", "value_in", "cot_in", "layer_in", "dq_out", "own", "home", "weight",
         )
         for name, ref in zip(fixed + names, refs, strict=True):
             setattr(self, name, ref)
@@ -124,6 +130,7 @@
         for head in range(self.heads):
             self.send_far(head)
         self.turn()
+        self.allow()
         for kind, index in self.plan:
             getattr(self, kind)(index)
         self.finish()
@@ -187,17 +194,13 @@
             self.sum_send.at[c], self.sum_recv.at[c], tp=flip(self.tp, 1),
         )
 
-    def result_copies(self, head):
+    def result_copy(self, head, which):
         columns = pl.ds(head * HEAD_DIM, HEAD_DIM)
-        pairs = (
-            (self.dq.at[head], self.dq_out),
-            (self.dkv.at[head, 0], self.dk_out),
-            (self.dkv.at[head, 1], self.dv_out),
-        )
-        return [
-            pltpu.make_async_copy(src, dst.at[:, columns], self.store_sem.at[head, i])
-            for i, (src, dst) in enumerate(pairs)
-        ]
+        src, dst = (
+            (self.dq.at[head], self.dq_out.at[:, columns]),
+            (self.dkv.at[head], self.own.at[head]),
+        )[which]
+        return pltpu.make_async_copy(src, dst, self.store_sem.at[head, which])
 
 
     def start(self):
@@ -225,11 +228,48 @@
         pl.semaphore_wait(barrier, self.spans + 1)
 
     def send_far(self, head):
-        def send(to, carry):
-            self.far_copy(head, to, self.me).start()
-            return carry
-
-        lax.fori_loop(self.me + 1, self.spans, send, 0)
+        def send(step, carry):
+            self.far_copy(head, self.spans - 1 - step, self.me).start()
+            return carry
+
+        lax.fori_loop(0, self.spans - 1 - self.me, send, 0)
+
+    def allow(self):
+        spans, rows, heads = self.spans, self.rows, self.heads
+        blocks = rows // KEY_BLOCK
+        entries = self.chosen.shape[1]
+        first = self.me * blocks
+        group = lax.div(first, 128) * 128
+        shift = first - group
+        row = lax.broadcasted_iota(jnp.int32, (128, rows), 0) - shift
+        of = lax.broadcasted_iota(jnp.int32, (128, rows), 1) // KEY_BLOCK
+        spread = jnp.where(row == of, 1.0, 0.0).astype(jnp.bfloat16)
+        wide = (spans * CAP, 128)
+        slot = lax.broadcasted_iota(jnp.int32, wide, 0)
+        base = slot // CAP * blocks
+        lane = lax.broadcasted_iota(jnp.int32, (1, 128), 1)
+        here = (lane >= shift) & (lane < shift + blocks)
+        for head in range(heads):
+            at = pl.ds(pl.multiple_of(group, 128), 128)
+            own = [jnp.where(here, self.chosen[head, e : e + 1, at], -1) for e in range(entries)]
+            low = jnp.full(wide, spans * blocks, jnp.int32)
+            high = jnp.full(wide, -2, jnp.int32)
+            for entry in own:
+                inside = (entry >= base) & (entry < base + blocks)
+                low = jnp.minimum(low, jnp.where(inside, entry, spans * blocks))
+                high = jnp.maximum(high, jnp.where(inside, entry, -2))
+            low = jnp.min(low, axis=1, keepdims=True)
+            high = jnp.max(high, axis=1, keepdims=True)
+            high = jnp.where(high == low, -2, high)
+            wanted = jnp.where(slot % CAP == 0, low, high)
+            hit = own[0] == wanted
+            for entry in own[1:]:
+                hit = hit | (entry == wanted)
+            hits = jnp.where(hit, 1.0, 0.0).astype(jnp.bfloat16)
+            used = dot(hits, spread, NN)
+            minus = self.sums[head : head + 1, :] * -LOG2E
+            self.bias[head, : spans * CAP, :] = jnp.where(used > 0.5, minus, NEVER)
+            self.bias[head, spans * CAP :, :] = jnp.broadcast_to(minus, (8, rows))
 
     def turn(self):
         self.load(4).wait()
@@ -265,16 +305,19 @@
             return carry
 
         lax.fori_loop(0, self.me, arrived, 0)
+        far_k = self.far[head, : self.spans - 1, 0].reshape(self.far_rows, HEAD_DIM)
+        self.key_turned[...] = far_k.T
+        self.acc[...] = jnp.zeros_like(self.acc)
         lax.fori_loop(0, self.tiles, functools.partial(self.attend_tile, head), 0)
-        self.dq_copy(head, self.tiles - 1).start()
-        for copy in self.result_copies(head):
-            copy.start()
+        self.result_copy(head, 0).start()
+        self.result_copy(head, 1).start()
         scale = HEAD_DIM ** (-0.5)
         spans = self.spans
         shape = (spans - 1, CAP * KEY_BLOCK, HEAD_DIM)
         self.back[head, : spans - 1, 0] = (scale * self.acc[0]).astype(jnp.bfloat16).reshape(shape)
         self.back[head, : spans - 1, 1] = self.acc[1].astype(jnp.bfloat16).reshape(shape)
 
+    def send_home(self, head):
         def send(to, carry):
             self.back_copy(head, to, self.me).start()
             return carry
@@ -317,27 +360,17 @@
         far_low = far_p.astype(jnp.bfloat16)
         own_low = own_p.astype(jnp.bfloat16)
 
-        far_q = dot(far_d, far_k, TN)
+        turned = dot(self.key_turned[...], far_d, NN) + jnp.concatenate(
+            [dot(key[r, :], own_d[:, r], TN) for r in parts], axis=1
+        )
+        self.dq[head, rows, :] = (scale * turned).T.astype(jnp.bfloat16)
         for r in parts:
-            dq = far_q[r, :] + dot(own_d[:, r], key[r, :], TN)
             here = pl.ds(pl.multiple_of(step * tile + r.start, SUB), SUB)
-            self.dq[head, here, :] = (scale * dq).astype(jnp.bfloat16)
             self.dkv[head, 0, here, :] = scale * dot(own_d[:, r], query[r, :], NN)
             self.dkv[head, 1, here, :] = dot(own_low[:, r], cot[r, :], NN)
-        step_k = dot(far_d, query, NN)
-        step_v = dot(far_low, cot, NN)
-
-        @pl.when(step == 0)
-        def _():
-            self.acc[0] = step_k
-            self.acc[1] = step_v
-
-        @pl.when(step > 0)
-        def _():
-            self.acc[0] += step_k
-            self.acc[1] += step_v
-            self.dq_copy(head, step - 1).start()
-
+        self.acc[0] += dot(far_d, query, NN)
+        self.acc[1] += dot(far_low, cot, NN)
+        self.dq_copy(head, step).start()
         return carry
 
     def source(self, kind, head):
@@ -383,34 +416,43 @@
 
         lax.fori_loop(0, self.pieces, one, 0)
 
-    def relay(self, c):
-        part = getattr(self, f"part{c}")
-        bit = lax.rem(self.me, 2)
-        low, ranges = 0, []
+    def ranges(self):
+        low, out = 0, []
         for stage in range(1, self.stages):
             half = (self.pieces - low) // 2
-            ranges.append((stage, low, half))
+            out.append((stage, low, half))
             low += half
-
-        def total(slot):
-            self.give_copy(c, 0, slot).wait_recv()
-            value = part[slot, bit] + getattr(self, f"got{c}_0")[slot].astype(jnp.float32)
-            for stage, first, half in ranges:
-                if slot >= first + half:
-                    at = slot - half - first
-                    self.give_copy(c, stage, at).wait_recv()
-                    got = getattr(self, f"got{c}_{stage}")
-                    value = value + got[at].astype(jnp.float32)
-                else:
-                    break
-            return value
-
+        return out
+
+    def total(self, c, slot):
+        part = getattr(self, f"part{c}")
+        self.give_copy(c, 0, slot).wait_recv()
+        value = part[slot, lax.rem(self.me, 2)]
+        value = value + getattr(self, f"got{c}_0")[slot].astype(jnp.float32)
+        for stage, first, half in self.ranges():
+            if slot < first + half:
+                break
+            at = slot - half - first
+            self.give_copy(c, stage, at).wait_recv()
+            value = value + getattr(self, f"got{c}_{stage}")[at].astype(jnp.float32)
+        return value
+
+    def relay(self, c, ranges):
         for stage, first, half in ranges:
             for slot in range(first, first + half):
-                getattr(self, f"give{c}_{stage}")[slot - first] = total(slot).astype(jnp.bfloat16)
+                give = getattr(self, f"give{c}_{stage}")
+                give[slot - first] = self.total(c, slot).astype(jnp.bfloat16)
                 self.give_copy(c, stage, slot - first).start()
+
+    def first(self, c):
+        self.relay(c, self.ranges()[:1])
+
+    def rest(self, c):
+        self.relay(c, self.ranges()[1:])
+
+    def settle(self, c):
         final = getattr(self, f"sum{c}")
-        final[...] = total(self.pieces - 1).reshape(final.shape)
+        final[...] = self.total(c, self.pieces - 1).reshape(final.shape)
         self.sum_copy(c).start()
         for at, (kind, head) in enumerate(self.chunks[c]):
             self.put(self.tp, kind, head, final[0, :, at * HEAD_DIM : (at + 1) * HEAD_DIM])
@@ -459,11 +501,11 @@
                 return carry
 
             lax.fori_loop(0, self.tiles, sent, 0)
-            for copy in self.result_copies(head):
-                copy.wait()
-
-
-def whole_step(bias, picked, query, key, value, cot, layer, tp_count):
+            self.result_copy(head, 0).wait()
+            self.result_copy(head, 1).wait()
+
+
+def whole_step(chosen, sums, picked, query, key, value, cot, layer, tp_count):
     spans, heads = picked.shape[:2]
     rows = query.shape[0]
     plan = Kernel(spans, tp_count, heads, rows, layer.shape[1])
@@ -476,22 +518,23 @@
         functools.partial(plan.body, names),
         out_shape=(
             jax.ShapeDtypeStruct((rows, wide), jnp.bfloat16),
-            jax.ShapeDtypeStruct((rows, wide), jnp.float32),
-            jax.ShapeDtypeStruct((rows, wide), jnp.float32),
+            jax.ShapeDtypeStruct((heads, 2, rows, HEAD_DIM), jnp.float32),
             jax.ShapeDtypeStruct((spans, heads, 2, CAP * KEY_BLOCK, HEAD_DIM), jnp.bfloat16),
             jax.ShapeDtypeStruct((plan.slice, tp_count * wide), jnp.float32),
         ),
-        in_specs=[vmem] + [hbm] * 6,
-        out_specs=(hbm, hbm, hbm, hbm, vmem),
+        in_specs=[vmem] * 3 + [hbm] * 5,
+        out_specs=(hbm, hbm, hbm, vmem),
         scratch_shapes=list(scratch.values()),
         compiler_params=pltpu.CompilerParams(
             collective_id=0, has_side_effects=True, vmem_limit_bytes=67043328
         ),
         name="whole_step",
-    )(bias, picked, query, key, value, cot, layer)
-
-
-def prepare_body(chosen, sums, key_in, value_in, ids, picked, bias, key, value, found, marks, sem, mark_sem):
+    )(chosen, sums, picked, query, key, value, cot, layer)
+
+
+def prepare_body(
+    chosen, key_in, value_in, ids, picked, key, value, found, marks, sem, mark_sem
+):
     loads = [
         pltpu.make_async_copy(src, dst, sem.at[i])
         for i, (src, dst) in enumerate(((key_in, key), (value_in, value)))
@@ -499,49 +542,23 @@
     for load in loads:
         load.start()
     spans, heads = picked.shape[:2]
-    rows = sums.shape[1]
-    blocks = rows // KEY_BLOCK
-    entries = chosen.shape[2]
+    blocks = key.shape[0] // KEY_BLOCK
+    count = chosen.shape[2]
     first = lax.axis_index("kv") * blocks
+    asker = lax.broadcasted_iota(jnp.int32, (spans, count), 1) // blocks
+    asks = asker == lax.broadcasted_iota(jnp.int32, (spans, count), 0)
+    lane = lax.broadcasted_iota(jnp.int32, (spans, 128), 1)
     for head in range(heads):
         lists = chosen[head] - first
         mine = (lists >= 0) & (lists < blocks)
-        low = jnp.where(mine, lists, blocks).reshape(spans, blocks, entries)
-        high = jnp.where(mine, lists, 0).reshape(spans, blocks, entries)
-        low = jnp.min(jnp.min(low, axis=1), axis=1, keepdims=True)
-        high = jnp.max(jnp.max(high, axis=1), axis=1, keepdims=True)
+        low = jnp.min(jnp.where(mine, lists, blocks), axis=0, keepdims=True)
+        high = jnp.max(jnp.where(mine, lists, 0), axis=0, keepdims=True)
+        low = jnp.min(jnp.where(asks, low, blocks), axis=1, keepdims=True)
+        high = jnp.max(jnp.where(asks, high, 0), axis=1, keepdims=True)
         low = jnp.where(low == blocks, 0, low)
-        lane = lax.broadcasted_iota(jnp.int32, (spans, 128), 1)
         found[head] = jnp.where(lane == 0, low, high)
     copy = pltpu.make_async_copy(found, marks, mark_sem)
     copy.start()
-
-    none = spans * blocks
-    row = lax.broadcasted_iota(jnp.int32, (blocks, rows), 0)
-    spread = jnp.where(
-        lax.broadcasted_iota(jnp.int32, (blocks, rows), 1) // KEY_BLOCK == row, 1.0, 0.0
-    ).astype(jnp.bfloat16)
-    for head in range(heads):
-        own = chosen[head, pl.ds(pl.multiple_of(first, blocks), blocks), :]
-        lane = lax.broadcasted_iota(jnp.int32, (1, spans * CAP), 1)
-        wanted = jnp.full((1, spans * CAP), -2, jnp.int32)
-        for span in range(spans):
-            inside = (own >= span * blocks) & (own < (span + 1) * blocks)
-            low = jnp.min(jnp.where(inside, own, none), axis=0, keepdims=True)
-            low = jnp.min(low, axis=1, keepdims=True)
-            high = jnp.max(jnp.where(inside, own, -2), axis=0, keepdims=True)
-            high = jnp.max(high, axis=1, keepdims=True)
-            high = jnp.where(high == low, -2, high)
-            wanted = jnp.where(lane == span * CAP, low, wanted)
-            wanted = jnp.where(lane == span * CAP + 1, high, wanted)
-        hit = own[:, 0:1] == wanted
-        for entry in range(1, entries):
-            hit = hit | (own[:, entry : entry + 1] == wanted)
-        hit = jnp.where(hit, 1.0, 0.0).astype(jnp.bfloat16)
-        used = dot(hit, spread, TN)
-        minus = sums[head : head + 1, :] * -LOG2E
-        bias[head, : spans * CAP, :] = jnp.where(used > 0.5, minus, NEVER)
-        bias[head, spans * CAP :, :] = jnp.broadcast_to(minus, (8, rows))
 
     copy.wait()
     for load in loads:
@@ -562,8 +579,8 @@
     lax.fori_loop(0, spans, one, 0)
 
 
-def prepare(chosen, sums, key, value, spans):
-    heads, rows = sums.shape
+def prepare(chosen, key, value, spans):
+    heads = chosen.shape[0]
     vmem = pl.BlockSpec(memory_space=pltpu.VMEM)
     smem = pl.BlockSpec(memory_space=pltpu.SMEM)
     hbm = pl.BlockSpec(memory_space=pl.ANY)
@@ -572,10 +589,9 @@
         out_shape=(
             jax.ShapeDtypeStruct((CAP, heads * spans), jnp.int32),
             jax.ShapeDtypeStruct((spans, heads, 2, CAP * KEY_BLOCK, HEAD_DIM), jnp.bfloat16),
-            jax.ShapeDtypeStruct((heads, spans * CAP + 8, rows), jnp.float32),
         ),
-        in_specs=[vmem, vmem, hbm, hbm],
-        out_specs=(smem, vmem, vmem),
+        in_specs=[vmem, hbm, hbm],
+        out_specs=(smem, vmem),
         scratch_shapes=[
             pltpu.VMEM(key.shape, key.dtype),
             pltpu.VMEM(value.shape, value.dtype),
@@ -585,56 +601,75 @@
             pltpu.SemaphoreType.DMA,
         ],
         name="prepare_blocks",
-    )(chosen, sums, key, value)
-
-
-def land_body(ids_ref, own_k, own_v, home, out_k, out_v):
+    )(chosen, key, value)
+
+
+def land_body(
+    ids, own_in, home_in, dq_in, weight_in, dq_out, out_k, out_v, weight_out,
+    own, home, dq, weight, load_sem, store_sem,
+):
+    heads = own.shape[0]
     spans = home.shape[0]
-    head = pl.program_id(0)
-    out_k[...] = own_k[...]
-    out_v[...] = own_v[...]
-
-    def one(span, carry):
-        for slot in range(CAP):
-            start = pl.multiple_of(ids_ref[slot, head * spans + span] * KEY_BLOCK, KEY_BLOCK)
-            rows = pl.ds(start, KEY_BLOCK)
-            at = slice(slot * KEY_BLOCK, (slot + 1) * KEY_BLOCK)
-            out_k[rows, :] += home[span, 0, 0, at, :].astype(jnp.float32)
-            out_v[rows, :] += home[span, 0, 1, at, :].astype(jnp.float32)
-        return carry
-
-    lax.fori_loop(lax.axis_index("kv") + 1, spans, one, 0)
-
-
-def land(ids, own_k, own_v, home):
-    spans, heads = home.shape[:2]
-    rows = own_k.shape[0]
+    parts = [(head, kind) for head in range(heads) for kind in range(2)]
+    loads, stores = [], []
+    for head, kind in parts:
+        columns = pl.ds(head * HEAD_DIM, HEAD_DIM)
+        loads.append((own_in.at[head, kind], own.at[head, kind]))
+        stores.append((own.at[head, kind], (out_k, out_v)[kind].at[:, columns]))
+    loads += [(dq_in, dq), (weight_in, weight)]
+    stores += [(dq, dq_out), (weight, weight_out)]
+    first = pltpu.make_async_copy(home_in, home, load_sem.at[len(loads)])
+    first.start()
+    loads = [pltpu.make_async_copy(*pair, load_sem.at[i]) for i, pair in enumerate(loads)]
+    stores = [pltpu.make_async_copy(*pair, store_sem.at[i]) for i, pair in enumerate(stores)]
+    for load in loads:
+        load.start()
+    first.wait()
+    for i, load in enumerate(loads):
+        load.wait()
+        if i < len(parts):
+            head, kind = parts[i]
+
+            def one(span, carry, head=head, kind=kind):
+                for slot in range(CAP):
+                    start = ids[slot, head * spans + span] * KEY_BLOCK
+                    rows = pl.ds(pl.multiple_of(start, KEY_BLOCK), KEY_BLOCK)
+                    at = slice(slot * KEY_BLOCK, (slot + 1) * KEY_BLOCK)
+                    own[head, kind, rows, :] += home[span, head, kind, at, :].astype(jnp.float32)
+                return carry
+
+            lax.fori_loop(lax.axis_index("kv") + 1, spans, one, 0)
+        stores[i].start()
+    for store in stores:
+        store.wait()
+
+
+def land(ids, own, home, dq, weight):
+    heads, _, rows, _ = own.shape
+    smem = pl.BlockSpec(memory_space=pltpu.SMEM)
+    hbm = pl.BlockSpec(memory_space=pl.ANY)
     whole = jax.ShapeDtypeStruct((rows, heads * HEAD_DIM), jnp.float32)
-    column = pl.BlockSpec((rows, HEAD_DIM), lambda h: (0, h))
+    like = [jax.ShapeDtypeStruct(x.shape, x.dtype) for x in (dq, weight)]
     return pl.pallas_call(
         land_body,
-        grid=(heads,),
-        out_shape=(whole, whole),
-        in_specs=[
-            pl.BlockSpec(memory_space=pltpu.SMEM),
-            column,
-            column,
-            pl.BlockSpec((spans, 1) + home.shape[2:], lambda h: (0, h, 0, 0, 0)),
-        ],
-        out_specs=(column, column),
+        out_shape=(like[0], whole, whole, like[1]),
+        in_specs=[smem] + [hbm] * 4,
+        out_specs=(hbm,) * 4,
+        scratch_shapes=[pltpu.VMEM(x.shape, x.dtype) for x in (own, home, dq, weight)]
+        + [pltpu.SemaphoreType.DMA((2 * heads + 3,)), pltpu.SemaphoreType.DMA((2 * heads + 2,))],
         name="land_blocks",
-    )(ids, own_k, own_v, home)
+    )(ids, own, home, dq, weight)
 
 
 def local(query_rows, key_rows, value_rows, log_sums, cotangent, layer_input, chosen):
     kv_count = lax.axis_size("kv")
     tp_count = lax.axis_size("tp")
-    ids, picked, bias = prepare(chosen, log_sums, key_rows, value_rows, kv_count)
-    dq, own_k, own_v, home, weight = whole_step(
-        bias, picked, query_rows, key_rows, value_rows, cotangent, layer_input, tp_count
+    chosen = jnp.swapaxes(chosen, 1, 2)
+    ids, picked = prepare(chosen, key_rows, value_rows, kv_count)
+    dq, own, home, weight = whole_step(
+        chosen, log_sums, picked, query_rows, key_rows, value_rows, cotangent, layer_input, tp_count
     )
-    grad_keys, grad_values = land(ids, own_k, own_v, home)
-    return dq, grad_keys, grad_values, weight
+    return land(ids, own, home, dq, weight)
 
 
 def solution(mesh):

time: 103 us -> 86.5 us (0.84)
  Pallas kernels: 97.1 us -> 85.7 us
  local copies, waits for them, and re-layouts: 4.6 us -> 0 us
    pallas_call x1, Pallas kernels: 85.8 us -> 74.1 us  [whole_step(): pl.pallas_call(functools.partial(plan.body, names), out_shape=(jax.ShapeD...]
    unnamed x7 -> x0, local copies, waits for them, and re-layouts: 4.6 us -> none
where the time goes in v1:
time: 86.5 us; the launch traced here: 86.3 us
  Pallas kernels  85.7 us (99%)
    pallas_call x1, Pallas kernels, whole_step(): pl.pallas_call(functools.partial(plan.body, names), out_shape=(jax.ShapeD...  74.1 us
    pallas_call x1, Pallas kernels, land(): pl.pallas_call(land_body, out_shape=(like[0], whole, whole, like[1]), in_...  7.62 us
    pallas_call x1, Pallas kernels, prepare(): pl.pallas_call(prepare_body, out_shape=(jax.ShapeDtypeStruct((CAP, heads...  3.98 us

profile of v1, /device:TPU:0, one launch (start us, length us, event | category | flops | bytes accessed | tf_op | source)
XLA Modules:
  0.0 86.3 jit_solution(16904104387174629651)
XLA Ops:
  0.6 4.0 %prepare_blocks.1 = (s32[2,24]{1,0:T(2,128)}, bf16[8,3,2,64,128]{4,3,2,1,0:T(8,128)(2,1)}) custom-call(s32[3,12,512]{2,1,0:T(8,128)} %bitcast.1, bf16[2048,384]{1,0:T(8,128)(2,1)} %refs_4_.1, bf16[2048,384]{1,0:T(8,128)(2,1)} %refs_5_.1), custom_call_target="tpu_custom_call" | custom-call | tf_op jit(solution)/shard_map/prepare_blocks/pallas_call | solution.py:587
  4.6 74.1 %whole_step.1 = (bf16[2048,384]{1,0:T(8,128)(2,1)}, f32[3,2,2048,128]{3,2,1,0:T(8,128)}, bf16[8,3,2,64,128]{4,3,2,1,0:T(8,128)(2,1)}, f32[128,1536]{1,0:T(8,128)}) custom-call(s32[3,12,512]{2,1,0:T(8,128)} %bitcast.2, f32[3,2048]{1,0:T(4,128)} %refs_1_.1, bf16[8,3,2,64,128]{4,3,2,1,0:T(8,128)(2,1)} %get-tuple-element.11.refs_2_, bf16[2048,384]{1,0:T(8,128)(2,1)} %refs_3_.1, ...), custom_call_target="tpu_custom_call" | custom-call | tf_op jit(solution)/shard_map/whole_step/pallas_call | solution.py:517
  78.7 7.6 %land_blocks.1 = (bf16[2048,384]{1,0:T(8,128)(2,1)}, f32[2048,384]{1,0:T(8,128)}, f32[2048,384]{1,0:T(8,128)}, f32[128,1536]{1,0:T(8,128)}) custom-call(s32[2,24]{1,0:T(2,128)} %get-tuple-element.10.ids, f32[3,2,2048,128]{3,2,1,0:T(8,128)} %get-tuple-element.12.own_in, bf16[8,3,2,64,128]{4,3,2,1,0:T(8,128)(2,1)} %get-tuple-element.13.home_in, ...), custom_call_target="tpu_custom_call" | custom-call | tf_op jit(solution)/shard_map/land_blocks/pallas_call | solution.py:653

commit v2 on v1

--- a/solution.py
+++ b/solution.py
@@ -29,9 +29,9 @@
 
 
 def chunk_plan(heads):
-    own = [("own", head) for head in range(heads)]
-    came = [("came", head) for head in range(heads)]
-    return [[one] for one in own[:-1]] + [[own[-1], came[0]]] + [[one] for one in came[1:]]
+    own = [[("own", head)] for head in range(heads)]
+    came = [[("came", head)] for head in range(heads)]
+    return own[:1] + [own[1] + came[0]] + own[2:] + came[1:]
 
 
 def step_plan(heads):
@@ -43,14 +43,14 @@
     plan += [("rest", chunk) for chunk in range(heads - 2)]
     last = 2 * heads - 2
     for chunk in range(heads, last + 1):
-        plan += [("product", chunk), ("first", chunk - 1)]
+        plan.append(("product", chunk))
         if chunk == heads:
-            plan.append(("rest", heads - 2))
+            plan += [("first", heads - 1), ("rest", heads - 2)]
             plan += [("settle", early) for early in range(heads - 1)]
         else:
             plan.append(("settle", chunk - 2))
-        plan.append(("rest", chunk - 1))
-    return plan + [("first", last), ("settle", last - 1), ("rest", last), ("settle", last)]
+        plan += [("rest", chunk - 1), ("first", chunk)]
+    return plan + [("settle", last - 1), ("rest", last), ("settle", last)]
 
 
 class Kernel:
@@ -58,8 +58,9 @@
         self.spans, self.tp_count, self.heads = spans, tp_count, heads
         self.rows, self.features = rows, features
         self.far_rows = (spans - 1) * CAP * KEY_BLOCK
-        self.tile = 1024 if self.far_rows <= 512 else 256
-        self.tiles = rows // self.tile
+        self.tile = 1024 if self.far_rows <= 512 else 128
+        self.unit = min(self.tile, 512)
+        self.units = rows // self.unit
         self.slice = features // spans
         self.pieces = spans // 2
         self.chunks = chunk_plan(heads)
@@ -77,26 +78,24 @@
             key=pltpu.VMEM((rows, wide), bf),
             value=pltpu.VMEM((rows, wide), bf),
             cot=pltpu.VMEM((rows, wide), bf),
-            layer=pltpu.VMEM((rows, self.features), bf),
+            layer=pltpu.VMEM((4, rows, HEAD_DIM), bf),
+            layer_sem=dma((4,)),
             turned=pltpu.VMEM((spans, 2, self.slice, rows), bf),
             far=pltpu.VMEM((heads, spans, 2, span_rows, HEAD_DIM), bf),
             back=pltpu.VMEM((heads, spans, 2, span_rows, HEAD_DIM), bf),
             acc=pltpu.VMEM((2, self.far_rows, HEAD_DIM), f32),
             key_turned=pltpu.VMEM((HEAD_DIM, self.far_rows), bf),
             bias=pltpu.VMEM((heads, spans * CAP + 8, rows), f32),
-            dq=pltpu.VMEM((heads, rows, HEAD_DIM), bf),
             came=pltpu.VMEM((heads, rows, HEAD_DIM), bf),
-            dkv=pltpu.VMEM((heads, 2, rows, HEAD_DIM), f32),
-            load_sem=dma((6,)),
-            store_sem=dma((heads, 2)),
+            load_sem=dma((4,)),
             far_send=dma((heads, spans)),
             far_recv=dma((heads, spans)),
             back_send=dma((heads, spans)),
             back_recv=dma((heads, spans)),
             turn_send=dma((spans,)),
             turn_recv=dma((spans,)),
-            dq_send=dma((heads, self.tiles)),
-            dq_recv=dma((heads, self.tiles)),
+            dq_send=dma((heads, self.units)),
+            dq_recv=dma((heads, self.units)),
         )
         count = len(self.chunks)
         for c, chunk in enumerate(self.chunks):
@@ -119,7 +118,7 @@
 
     def body(self, names, *refs):
         fixed = (
-            "chosen", "sums", "picked", "query_in", "key_in", "value_in", "cot_in", "layer_in", "dq_out", "own", "home", "weight",
+            "chosen", "sums", "picked", "query_in", "key_in", "value_in", "cot_in", "layer_in", "dq", "own", "home", "weight",
         )
         for name, ref in zip(fixed + names, refs, strict=True):
             setattr(self, name, ref)
@@ -142,10 +141,16 @@
             (self.value_in, self.value),
             (self.query_in, self.query),
             (self.cot_in, self.cot),
-            (self.layer_in, self.layer),
         )
         src, dst = pairs[which]
         return pltpu.make_async_copy(src, dst, self.load_sem.at[which])
+
+    def layer_copy(self, group):
+        columns = pl.ds(pl.multiple_of(group * HEAD_DIM, HEAD_DIM), HEAD_DIM)
+        slot = lax.rem(group, 4)
+        return pltpu.make_async_copy(
+            self.layer_in.at[:, columns], self.layer.at[slot], self.layer_sem.at[slot]
+        )
 
     def remote(self, src, dst, send, recv, **to):
         return pltpu.make_async_remote_copy(
@@ -172,7 +177,7 @@
         )
 
     def dq_copy(self, head, tile):
-        rows = pl.ds(pl.multiple_of(tile * self.tile, self.tile), self.tile)
+        rows = pl.ds(pl.multiple_of(tile * self.unit, self.unit), self.unit)
         return self.remote(
             self.dq.at[head, rows], self.came.at[head, rows],
             self.dq_send.at[head, tile], self.dq_recv.at[head, tile],
@@ -194,18 +199,12 @@
             self.sum_send.at[c], self.sum_recv.at[c], tp=flip(self.tp, 1),
         )
 
-    def result_copy(self, head, which):
-        columns = pl.ds(head * HEAD_DIM, HEAD_DIM)
-        src, dst = (
-            (self.dq.at[head], self.dq_out.at[:, columns]),
-            (self.dkv.at[head], self.own.at[head]),
-        )[which]
-        return pltpu.make_async_copy(src, dst, self.store_sem.at[head, which])
-
 
     def start(self):
-        for which in range(5):
+        for which in range(4):
             self.load(which).start()
+        for group in range(4):
+            self.layer_copy(group).start()
         barrier = pltpu.get_barrier_semaphore()
 
         def greet(step, carry):
@@ -272,19 +271,23 @@
             self.bias[head, spans * CAP :, :] = jnp.broadcast_to(minus, (8, rows))
 
     def turn(self):
-        self.load(4).wait()
         group = HEAD_DIM // self.slice
         step_rows = 512
+        last = self.features // HEAD_DIM
 
         def one(g, carry):
-            columns = pl.ds(pl.multiple_of(g * HEAD_DIM, HEAD_DIM), HEAD_DIM)
+            self.layer_copy(g).wait()
             for at in range(0, self.rows, step_rows):
-                block = self.layer[at : at + step_rows, columns].T
+                block = self.layer[lax.rem(g, 4), at : at + step_rows, :].T
                 for j in range(group):
                     self.turned[g * group + j, 0, :, at : at + step_rows] = block[
                         j * self.slice : (j + 1) * self.slice
                     ]
 
+            @pl.when(g + 4 < last)
+            def _():
+                self.layer_copy(g + 4).start()
+
             @pl.when(g > 0)
             def _():
                 for j in range(group):
@@ -292,7 +295,6 @@
 
             return carry
 
-        last = self.features // HEAD_DIM
         lax.fori_loop(0, last, one, 0)
         for which in range(4):
             self.load(which).wait()
@@ -308,9 +310,10 @@
         far_k = self.far[head, : self.spans - 1, 0].reshape(self.far_rows, HEAD_DIM)
         self.key_turned[...] = far_k.T
         self.acc[...] = jnp.zeros_like(self.acc)
-        lax.fori_loop(0, self.tiles, functools.partial(self.attend_tile, head), 0)
-        self.result_copy(head, 0).start()
-        self.result_copy(head, 1).start()
+        tile = self.tile if head else self.unit
+        lax.fori_loop(
+            0, self.rows // tile, functools.partial(self.attend_tile, head, tile), 0
+        )
         scale = HEAD_DIM ** (-0.5)
         spans = self.spans
         shape = (spans - 1, CAP * KEY_BLOCK, HEAD_DIM)
@@ -324,8 +327,8 @@
 
         lax.fori_loop(0, self.me, send, 0)
 
-    def attend_tile(self, head, step, carry):
-        tile, spans, far_rows = self.tile, self.spans, self.far_rows
+    def attend_tile(self, head, tile, step, carry):
+        spans, far_rows = self.spans, self.far_rows
         scale = HEAD_DIM ** (-0.5)
         columns = slice(head * HEAD_DIM, (head + 1) * HEAD_DIM)
         rows = pl.ds(pl.multiple_of(step * tile, tile), tile)
@@ -366,11 +369,13 @@
         self.dq[head, rows, :] = (scale * turned).T.astype(jnp.bfloat16)
         for r in parts:
             here = pl.ds(pl.multiple_of(step * tile + r.start, SUB), SUB)
-            self.dkv[head, 0, here, :] = scale * dot(own_d[:, r], query[r, :], NN)
-            self.dkv[head, 1, here, :] = dot(own_low[:, r], cot[r, :], NN)
+            self.own[head, 0, here, :] = scale * dot(own_d[:, r], query[r, :], NN)
+            self.own[head, 1, here, :] = dot(own_low[:, r], cot[r, :], NN)
         self.acc[0] += dot(far_d, query, NN)
         self.acc[1] += dot(far_low, cot, NN)
-        self.dq_copy(head, step).start()
+        count = tile // self.unit
+        for unit in range(count):
+            self.dq_copy(head, step * count + unit).start()
         return carry
 
     def source(self, kind, head):
@@ -395,7 +400,7 @@
                     self.dq_copy(head, tile).wait_recv()
                     return carry
 
-                lax.fori_loop(0, self.tiles, arrived, 0)
+                lax.fori_loop(0, self.units, arrived, 0)
         if c == 0:
 
             def turned(place, carry):
@@ -500,9 +505,7 @@
                 self.dq_copy(head, tile).wait_send()
                 return carry
 
-            lax.fori_loop(0, self.tiles, sent, 0)
-            self.result_copy(head, 0).wait()
-            self.result_copy(head, 1).wait()
+            lax.fori_loop(0, self.units, sent, 0)
 
 
 def whole_step(chosen, sums, picked, query, key, value, cot, layer, tp_count):
@@ -517,16 +520,16 @@
     return pl.pallas_call(
         functools.partial(plan.body, names),
         out_shape=(
-            jax.ShapeDtypeStruct((rows, wide), jnp.bfloat16),
-            jax.ShapeDtypeStruct((heads, 2, rows, HEAD_DIM), jnp.float32),
-            jax.ShapeDtypeStruct((spans, heads, 2, CAP * KEY_BLOCK, HEAD_DIM), jnp.bfloat16),
-            jax.ShapeDtypeStruct((plan.slice, tp_count * wide), jnp.float32),
+            pltpu.VMEM((heads, rows, HEAD_DIM), jnp.bfloat16),
+            pltpu.VMEM((heads, 2, rows, HEAD_DIM), jnp.float32),
+            pltpu.VMEM((spans, heads, 2, CAP * KEY_BLOCK, HEAD_DIM), jnp.bfloat16),
+            pltpu.VMEM((plan.slice, tp_count * wide), jnp.float32),
         ),
         in_specs=[vmem] * 3 + [hbm] * 5,
-        out_specs=(hbm, hbm, hbm, vmem),
+        out_specs=(vmem,) * 4,
         scratch_shapes=list(scratch.values()),
         compiler_params=pltpu.CompilerParams(
-            collective_id=0, has_side_effects=True, vmem_limit_bytes=67043328
+            collective_id=0, has_side_effects=True, vmem_limit_bytes=50 * 2**20
         ),
         name="whole_step",
     )(chosen, sums, picked, query, key, value, cot, layer)
@@ -588,7 +591,7 @@
         prepare_body,
         out_shape=(
             jax.ShapeDtypeStruct((CAP, heads * spans), jnp.int32),
-            jax.ShapeDtypeStruct((spans, heads, 2, CAP * KEY_BLOCK, HEAD_DIM), jnp.bfloat16),
+            pltpu.VMEM((spans, heads, 2, CAP * KEY_BLOCK, HEAD_DIM), jnp.bfloat16),
         ),
         in_specs=[vmem, hbm, hbm],
         out_specs=(smem, vmem),
@@ -604,59 +607,61 @@
     )(chosen, key, value)
 
 
-def land_body(
-    ids, own_in, home_in, dq_in, weight_in, dq_out, out_k, out_v, weight_out,
-    own, home, dq, weight, load_sem, store_sem,
-):
+def land_body(ids, own, home, dq, weight, dq_out, out_k, out_v, weight_out, result, sem):
     heads = own.shape[0]
     spans = home.shape[0]
-    parts = [(head, kind) for head in range(heads) for kind in range(2)]
-    loads, stores = [], []
-    for head, kind in parts:
+    stores = [(weight, weight_out)]
+    for head in range(heads):
         columns = pl.ds(head * HEAD_DIM, HEAD_DIM)
-        loads.append((own_in.at[head, kind], own.at[head, kind]))
-        stores.append((own.at[head, kind], (out_k, out_v)[kind].at[:, columns]))
-    loads += [(dq_in, dq), (weight_in, weight)]
-    stores += [(dq, dq_out), (weight, weight_out)]
-    first = pltpu.make_async_copy(home_in, home, load_sem.at[len(loads)])
-    first.start()
-    loads = [pltpu.make_async_copy(*pair, load_sem.at[i]) for i, pair in enumerate(loads)]
-    stores = [pltpu.make_async_copy(*pair, store_sem.at[i]) for i, pair in enumerate(stores)]
-    for load in loads:
-        load.start()
-    first.wait()
-    for i, load in enumerate(loads):
-        load.wait()
-        if i < len(parts):
-            head, kind = parts[i]
+        stores.append((dq.at[head], dq_out.at[:, columns]))
+    for head in range(heads):
+        columns = pl.ds(head * HEAD_DIM, HEAD_DIM)
+        stores.append((result.at[head, 0], out_k.at[:, columns]))
+        stores.append((result.at[head, 1], out_v.at[:, columns]))
+    stores = [pltpu.make_async_copy(*pair, sem.at[i]) for i, pair in enumerate(stores)]
+    ready = 1 + heads
+    for store in stores[:ready]:
+        store.start()
+    for head in range(heads):
+        for kind in range(2):
+            result[head, kind] = own[head, kind]
 
             def one(span, carry, head=head, kind=kind):
                 for slot in range(CAP):
                     start = ids[slot, head * spans + span] * KEY_BLOCK
                     rows = pl.ds(pl.multiple_of(start, KEY_BLOCK), KEY_BLOCK)
                     at = slice(slot * KEY_BLOCK, (slot + 1) * KEY_BLOCK)
-                    own[head, kind, rows, :] += home[span, head, kind, at, :].astype(jnp.float32)
+                    add = home[span, head, kind, at, :].astype(jnp.float32)
+                    result[head, kind, rows, :] += add
                 return carry
 
             lax.fori_loop(lax.axis_index("kv") + 1, spans, one, 0)
-        stores[i].start()
+            stores[ready + 2 * head + kind].start()
     for store in stores:
         store.wait()
 
 
 def land(ids, own, home, dq, weight):
     heads, _, rows, _ = own.shape
-    smem = pl.BlockSpec(memory_space=pltpu.SMEM)
+    wide = heads * HEAD_DIM
+    vmem = pl.BlockSpec(memory_space=pltpu.VMEM)
     hbm = pl.BlockSpec(memory_space=pl.ANY)
-    whole = jax.ShapeDtypeStruct((rows, heads * HEAD_DIM), jnp.float32)
-    like = [jax.ShapeDtypeStruct(x.shape, x.dtype) for x in (dq, weight)]
+    whole = jax.ShapeDtypeStruct((rows, wide), jnp.float32)
     return pl.pallas_call(
         land_body,
-        out_shape=(like[0], whole, whole, like[1]),
-        in_specs=[smem] + [hbm] * 4,
+        out_shape=(
+            jax.ShapeDtypeStruct((rows, wide), dq.dtype),
+            whole,
+            whole,
+            jax.ShapeDtypeStruct(weight.shape, weight.dtype),
+        ),
+        in_specs=[pl.BlockSpec(memory_space=pltpu.SMEM)] + [vmem] * 4,
         out_specs=(hbm,) * 4,
-        scratch_shapes=[pltpu.VMEM(x.shape, x.dtype) for x in (own, home, dq, weight)]
-        + [pltpu.SemaphoreType.DMA((2 * heads + 3,)), pltpu.SemaphoreType.DMA((2 * heads + 2,))],
+        scratch_shapes=[
+            pltpu.VMEM(own.shape, own.dtype),
+            pltpu.SemaphoreType.DMA((1 + 3 * heads,)),
+        ],
+        compiler_params=pltpu.CompilerParams(vmem_limit_bytes=16 * 2**20),
         name="land_blocks",
     )(ids, own, home, dq, weight)
 
@@ -666,6 +671,7 @@
     tp_count = lax.axis_size("tp")
     chosen = jnp.swapaxes(chosen, 1, 2)
     ids, picked = prepare(chosen, key_rows, value_rows, kv_count)
+    picked = pltpu.with_memory_space_constraint(picked, pltpu.VMEM)
     dq, own, home, weight = whole_step(
         chosen, log_sums, picked, query_rows, key_rows, value_rows, cotangent, layer_input, tp_count
     )

time: 86.5 us -> 80.2 us (0.927)
  Pallas kernels: 85.7 us -> 79.3 us
    pallas_call x2, Pallas kernels: 81.7 us -> 75.7 us  [the longest x1 71.6 us: whole_step(): pl.pallas_call(functools.partial(plan.body, names), out_shape=(pltpu.VMEM...]
where the time goes in v2:
time: 80.2 us; the launch traced here: 80 us
  Pallas kernels  79.3 us (99%)
    pallas_call x1, Pallas kernels, whole_step(): pl.pallas_call(functools.partial(plan.body, names), out_shape=(pltpu.VMEM...  71.6 us
    pallas_call x1, Pallas kernels, land(): pl.pallas_call(land_body, out_shape=(jax.ShapeDtypeStruct((rows, wide), d...  4.02 us
    pallas_call x1, Pallas kernels, prepare(): pl.pallas_call(prepare_body, out_shape=(jax.ShapeDtypeStruct((CAP, heads...  3.66 us

profile of v2, /device:TPU:0, one launch (start us, length us, event | category | flops | bytes accessed | tf_op | source)
XLA Modules:
  0.0 80.0 jit_solution(1318201797611728449)
XLA Ops:
  0.6 3.7 %prepare_blocks.1 = (s32[2,24]{1,0:T(2,128)}, bf16[8,3,2,64,128]{4,3,2,1,0:T(8,128)(2,1)S(1)}) custom-call(s32[3,12,512]{2,1,0:T(8,128)} %bitcast.1, bf16[2048,384]{1,0:T(8,128)(2,1)} %refs_4_.1, bf16[2048,384]{1,0:T(8,128)(2,1)} %refs_5_.1), custom_call_target="tpu_custom_call" | custom-call | tf_op jit(solution)/shard_map/prepare_blocks/pallas_call | solution.py:590
  4.3 0.0 copy-start
  4.3 71.6 %whole_step.1 = (bf16[3,2048,128]{2,1,0:T(8,128)(2,1)S(1)}, f32[3,2,2048,128]{3,2,1,0:T(8,128)S(1)}, bf16[8,3,2,64,128]{4,3,2,1,0:T(8,128)(2,1)S(1)}, f32[128,1536]{1,0:T(8,128)S(1)}) custom-call(s32[3,12,512]{2,1,0:T(8,128)} %bitcast.2, f32[3,2048]{1,0:T(4,128)} %refs_1_.1, bf16[8,3,2,64,128]{4,3,2,1,0:T(8,128)(2,1)S(1)} %get-tuple-element.11.refs_2_, ...), custom_call_target="tpu_custom_call" | custom-call | tf_op jit(solution)/shard_map/whole_step/pallas_call | solution.py:520
  76.0 0.0 copy-done
  76.0 4.0 %land_blocks.1 = (bf16[2048,384]{1,0:T(8,128)(2,1)}, f32[2048,384]{1,0:T(8,128)}, f32[2048,384]{1,0:T(8,128)}, f32[128,1536]{1,0:T(8,128)}) custom-call(s32[2,24]{1,0:T(2,128)S(1)} %copy-done, f32[3,2,2048,128]{3,2,1,0:T(8,128)S(1)} %get-tuple-element.12.own, bf16[8,3,2,64,128]{4,3,2,1,0:T(8,128)(2,1)S(1)} %get-tuple-element.13.home, ...), custom_call_target="tpu_custom_call" | custom-call | tf_op jit(solution)/shard_map/land_blocks/pallas_call | solution.py:650
Async XLA Ops:
  4.3 71.7 %copy-start = (s32[2,24]{1,0:T(2,128)S(1)}, s32[2,24]{1,0:T(2,128)}, u32[]{:S(2)}) copy-start(s32[2,24]{1,0:T(2,128)} %get-tuple-element.10.ids) | copy-start | bytes 580

commit v3 on v2

--- a/solution.py
+++ b/solution.py
@@ -37,7 +37,9 @@
 def step_plan(heads):
     plan = []
     for head in range(heads):
-        plan += [("attend", head), ("product", head), ("send_home", head)]
+        plan += [("attend", head), ("product", head)]
+        if head < heads - 1:
+            plan.append(("send_home", head))
         if head:
             plan.append(("first", head - 1))
     plan += [("rest", chunk) for chunk in range(heads - 2)]
@@ -45,6 +47,7 @@
     for chunk in range(heads, last + 1):
         plan.append(("product", chunk))
         if chunk == heads:
+            plan.append(("send_home", heads - 1))
             plan += [("first", heads - 1), ("rest", heads - 2)]
             plan += [("settle", early) for early in range(heads - 1)]
         else:

time: 80.2 us -> 81.6 us (1.017)
  Pallas kernels: 79.3 us -> 80.6 us
    pallas_call x1, Pallas kernels: 71.6 us -> 72.9 us  [whole_step(): pl.pallas_call(functools.partial(plan.body, names), out_shape=(pltpu.VMEM...]
where the time goes in v3:
time: 81.6 us; the launch traced here: 81.3 us
  Pallas kernels  80.6 us (99%)
    pallas_call x1, Pallas kernels, whole_step(): pl.pallas_call(functools.partial(plan.body, names), out_shape=(pltpu.VMEM...  72.9 us
    pallas_call x1, Pallas kernels, land(): pl.pallas_call(land_body, out_shape=(jax.ShapeDtypeStruct((rows, wide), d...  4.02 us
    pallas_call x1, Pallas kernels, prepare(): pl.pallas_call(prepare_body, out_shape=(jax.ShapeDtypeStruct((CAP, heads...  3.66 us

profile of v3, /device:TPU:0, one launch (start us, length us, event | category | flops | bytes accessed | tf_op | source)
XLA Modules:
  0.0 81.3 jit_solution(13114374308791328826)
XLA Ops:
  0.6 3.7 %prepare_blocks.1 = (s32[2,24]{1,0:T(2,128)}, bf16[8,3,2,64,128]{4,3,2,1,0:T(8,128)(2,1)S(1)}) custom-call(s32[3,12,512]{2,1,0:T(8,128)} %bitcast.1, bf16[2048,384]{1,0:T(8,128)(2,1)} %refs_4_.1, bf16[2048,384]{1,0:T(8,128)(2,1)} %refs_5_.1), custom_call_target="tpu_custom_call" | custom-call | tf_op jit(solution)/shard_map/prepare_blocks/pallas_call | solution.py:593
  4.3 0.0 copy-start
  4.3 72.9 %whole_step.1 = (bf16[3,2048,128]{2,1,0:T(8,128)(2,1)S(1)}, f32[3,2,2048,128]{3,2,1,0:T(8,128)S(1)}, bf16[8,3,2,64,128]{4,3,2,1,0:T(8,128)(2,1)S(1)}, f32[128,1536]{1,0:T(8,128)S(1)}) custom-call(s32[3,12,512]{2,1,0:T(8,128)} %bitcast.2, f32[3,2048]{1,0:T(4,128)} %refs_1_.1, bf16[8,3,2,64,128]{4,3,2,1,0:T(8,128)(2,1)S(1)} %get-tuple-element.11.refs_2_, ...), custom_call_target="tpu_custom_call" | custom-call | tf_op jit(solution)/shard_map/whole_step/pallas_call | solution.py:523
  77.2 0.0 copy-done
  77.2 4.0 %land_blocks.1 = (bf16[2048,384]{1,0:T(8,128)(2,1)}, f32[2048,384]{1,0:T(8,128)}, f32[2048,384]{1,0:T(8,128)}, f32[128,1536]{1,0:T(8,128)}) custom-call(s32[2,24]{1,0:T(2,128)S(1)} %copy-done, f32[3,2,2048,128]{3,2,1,0:T(8,128)S(1)} %get-tuple-element.12.own, bf16[8,3,2,64,128]{4,3,2,1,0:T(8,128)(2,1)S(1)} %get-tuple-element.13.home, ...), custom_call_target="tpu_custom_call" | custom-call | tf_op jit(solution)/shard_map/land_blocks/pallas_call | solution.py:653
Async XLA Ops:
  4.3 72.9 %copy-start = (s32[2,24]{1,0:T(2,128)S(1)}, s32[2,24]{1,0:T(2,128)}, u32[]{:S(2)}) copy-start(s32[2,24]{1,0:T(2,128)} %get-tuple-element.10.ids) | copy-start | bytes 580
